TPU v7x, 128 devices: a whole 4x4x4 slice. The times are simulated.
128 devices in a mesh: fs: 16 (over z, y), rep: 4 (over x), tp: 2 (over core).
Axes of the slice: x: 4, y: 4, z: 4, core: 2. Of those that a mesh axis runs over, the one named last changes fastest.
Arguments:
- normed_in: bfloat16 [98304, 2048], P(('fs', 'rep')), may hold values from -6 to 6
- cotan_rec: bfloat16 [98304, 2048], P(('fs', 'rep'), 'tp'), may hold values from -0.01953125 to 0.01953125
- cotan_gate: bfloat16 [98304, 2048], P(('fs', 'rep'), 'tp'), may hold values from -0.01953125 to 0.01953125
- factor_rec: bfloat16 [2048, 512], P('fs'), may hold values from -0.125 to 0.125
- factor_gate: bfloat16 [2048, 512], P('fs'), may hold values from -0.125 to 0.125
- first_rec: float32 [512, 2048], P('fs', 'tp'), may hold values from -6 to 6
- first_gate: float32 [512, 2048], P('fs', 'tp'), may hold values from -6 to 6
- second_rec: float32 [512, 2048], P('fs', 'tp'), may hold values from 0.25 to 4
- second_gate: float32 [512, 2048], P('fs', 'tp'), may hold values from 0.25 to 4
- master_rec: float32 [2048, 2048], P('fs', 'tp'), may hold values from -0.125 to 0.125
- master_gate: float32 [2048, 2048], P('fs', 'tp'), may hold values from -0.125 to 0.125
Outputs:
- update_rec: float32 [2048, 2048], P('fs', 'tp')
- update_gate: float32 [2048, 2048], P('fs', 'tp')
- new_first_rec: float32 [512, 2048], P('fs', 'tp')
- new_first_gate: float32 [512, 2048], P('fs', 'tp')
- new_second_rec: float32 [512, 2048], P('fs', 'tp')
- new_second_gate: float32 [512, 2048], P('fs', 'tp')
- copy_rec: bfloat16 [2048, 2048], P(None, 'tp')
- copy_gate: bfloat16 [2048, 2048], P(None, 'tp')
All inputs are finite; a program needn't handle non-finite values.
Results may differ from a plain program's by a relative error of at most 0.007.
Values may be sent and summed in bfloat16 or wider, within the bound.
A program may use at most 128 MiB of HBM per device.

v0:
```python
import jax
import jax.numpy as jnp
from jax import lax
from jax.sharding import PartitionSpec as P

DR = 2048
RANK = 512


beta_first = 0.8
beta_second = 0.9
scale_floor = 0.25
step_rate = 0.01


def in_one_piece(arrays, axis, dim, along):
    ends, at = ([], 0)
    for a in arrays[:-1]:
        at += a.shape[along]
        ends.append(at)
    both = jnp.concatenate(arrays, axis=along)
    return tuple(jnp.split(lax.all_gather(both, axis, axis=dim, tiled=True), ends, axis=along))


def in_blocks(x, dim, size):
    lengths = x.shape
    tiles = x.reshape(*lengths[:dim], size, lengths[dim] // size, *lengths[dim + 1 :])
    return jnp.moveaxis(tiles, dim, 0)


def summed_on_arrival(x, axis, dim):
    size = lax.axis_size(axis)
    tiles = lax.all_to_all(in_blocks(x, dim, size), axis, 0, 0, tiled=True)
    return jnp.sum(tiles.astype(jnp.float32), axis=0)


def side_by_side(arrays, axis, dim, along):
    both = jnp.concatenate(arrays, axis=along)
    filled, at, gathered = (summed_on_arrival(both, axis, dim), 0, [])
    for a in arrays:
        gathered.append(lax.slice_in_dim(filled, at, at + a.shape[along], axis=along))
        at += a.shape[along]
    return tuple(gathered)


def sent_to_all(x, axis):
    size = lax.axis_size(axis)
    return lax.all_to_all(jnp.broadcast_to(x[None], (size, *x.shape)), axis, 0, 0, tiled=True)


def over_copies(x, axis):
    return sent_to_all(x, axis).astype(jnp.float32).sum(axis=0)


def over_copies_2(x, axis):
    everything = sent_to_all(x, axis)
    return jnp.sum(everything, axis=0)


def together(arrays, axis):
    ends = [0]
    for a in arrays:
        ends.append(ends[-1] + a.size)
    subtotal = over_copies_2(jnp.concatenate([a.ravel() for a in arrays]), axis)
    return tuple((subtotal[b:e].reshape(a.shape) for a, b, e in zip(arrays, ends, ends[1:])))


def split_product(projected, cotan):
    upper = projected.astype(jnp.bfloat16)
    lower = (projected - upper.astype(jnp.float32)).astype(jnp.bfloat16)
    dims = (((0,), (0,)), ((), ()))
    return lax.dot_general(
        upper, cotan, dims, preferred_element_type=jnp.float32
    ) + lax.dot_general(lower, cotan, dims, preferred_element_type=jnp.float32)


def moments(low, first, second):
    new_first = beta_first * first + (1.0 - beta_first) * low
    new_second = beta_second * second + (1.0 - beta_second) * low * low
    return (new_first, new_second, new_first / jnp.sqrt(new_second))


def body(
    normed_in,
    cotan_rec,
    cotan_gate,
    factor_rec,
    factor_gate,
    first_rec,
    first_gate,
    second_rec,
    second_gate,
    master_rec,
    master_gate,
):
    wide_rec = factor_rec.astype(jnp.float32)
    wide_gate = factor_gate.astype(jnp.float32)
    pieces = in_one_piece((factor_rec, factor_gate), "fs", 0, 1)
    proj_rec = jnp.dot(normed_in, pieces[0], preferred_element_type=jnp.float32)
    proj_gate = jnp.dot(normed_in, pieces[1], preferred_element_type=jnp.float32)
    part_rec = split_product(proj_rec, cotan_rec)
    part_gate = split_product(proj_gate, cotan_gate)
    low_rec, low_gate = side_by_side(
        (part_rec.astype(jnp.bfloat16), part_gate.astype(jnp.bfloat16)), "fs", 0, 1
    )
    low_rec, low_gate = (
        over_copies(low_rec.astype(jnp.bfloat16), "rep").astype(jnp.float32),
        over_copies(low_gate.astype(jnp.bfloat16), "rep").astype(jnp.float32),
    )
    first_r, second_r, direc_rec = moments(low_rec, first_rec, second_rec)
    first_g, second_g, direc_gate = moments(low_gate, first_gate, second_gate)
    total_rec, total_gate = together(
        (jnp.sum(direc_rec * direc_rec), jnp.sum(direc_gate * direc_gate)), ("fs", "tp")
    )
    entries = float(RANK * DR)
    scale_rec = 1.0 / jnp.sqrt(total_rec / entries + scale_floor)
    scale_gate = 1.0 / jnp.sqrt(total_gate / entries + scale_floor)
    pieces = in_one_piece((direc_rec, direc_gate), "fs", 0, 1)
    upd_rec = jnp.dot(wide_rec, pieces[0])
    upd_gate = jnp.dot(wide_gate, pieces[1])
    upd_rec = upd_rec * scale_rec
    upd_gate = upd_gate * scale_gate
    copy_rec = (master_rec - step_rate * upd_rec).astype(jnp.bfloat16)
    copy_gate = (master_gate - step_rate * upd_gate).astype(jnp.bfloat16)
    whole_rec, whole_gate = in_one_piece((copy_rec, copy_gate), "fs", 0, 1)
    return (upd_rec, upd_gate, first_r, first_g, second_r, second_g, whole_rec, whole_gate)


def solution(mesh):
    return jax.shard_map(
        body,
        mesh=mesh,
        in_specs=(
            P(("fs", "rep"), None),
            P(("fs", "rep"), "tp"),
            P(("fs", "rep"), "tp"),
            P("fs", None),
            P("fs", None),
            P("fs", "tp"),
            P("fs", "tp"),
            P("fs", "tp"),
            P("fs", "tp"),
            P("fs", "tp"),
            P("fs", "tp"),
        ),
        out_specs=(
            P("fs", "tp"),
            P("fs", "tp"),
            P("fs", "tp"),
            P("fs", "tp"),
            P("fs", "tp"),
            P("fs", "tp"),
            P(None, "tp"),
            P(None, "tp"),
        ),
        check_vma=False,
    )
```

profile of v0, /device:TPU:0, one launch (start us, length us, event | category | flops | bytes accessed | tf_op | source)
XLA Modules:
  0.0 289.4 jit_solution(16741537438718456146)
XLA Ops:
  7.2 1.8 pad_maximum_fusion.2
  9.1 55.6 %all-gather.4.cloned.1.call-done = bf16[2048,1024]{1,0:T(8,128)(2,1)} async-done(((bf16[128,1024]{1,0:T(8,128)(2,1)}), bf16[2048,1024]{1,0:T(8,128)(2,1)}) %all-gather.4.cloned.1.call-update) | async-done | bytes 4194320 | tf_op jit(solution)/shard_map/all_gather | solution.py:22
  64.7 6.4 %convolution_bitcast_fusion.1 = f32[1536,512]{0,1:T(8,128)S(1)} fusion(bf16[1536,2048]{1,0:T(8,128)(2,1)} %param.11, bf16[2048,1024]{1,0:T(8,128)(2,1)} %all-gather.4.cloned.1.call-done), kind=kOutput, calls=%fused_computation.1 | convolution fusion | flops 3221225472 | bytes 11534336 | tf_op jit(solution)/shard_map/dot_general | solution.py:99
  71.2 1.8 fusion.6
  73.0 1.8 add_convert_fusion.1
  75.2 3.5 %convolution_bitcast_fusion = f32[1536,512]{0,1:T(8,128)S(1)} fusion(bf16[1536,2048]{1,0:T(8,128)(2,1)S(1)} %bitcast.23, bf16[2048,1024]{1,0:T(8,128)(2,1)S(1)} %copy-done.10), kind=kOutput, calls=%fused_computation | convolution fusion | flops 3221225472 | bytes 11534336 | tf_op jit(solution)/shard_map/dot_general | solution.py:100
  78.7 1.8 fusion.7
  80.5 1.8 add_convert_fusion
  82.6 33.4 %all_to_all.21 = bf16[16,32,2048]{2,1,0:T(8,128)(2,1)} all-to-all(bf16[16,32,2048]{2,1,0:T(8,128)(2,1)S(1)} %bitcast.21), channel_id=1, replica_groups=mesh['fs'=16,'rep'=4,'tp'=2] {'fs'}, dimensions={0} | all-to-all | bytes 4194304 | tf_op jit(solution)/shard_map/all_to_all | solution.py:33
  116.0 2.1 reduce.1
  118.1 10.9 %all_to_all.22 = bf16[4,32,1024]{2,1,0:T(8,128)(2,1)S(1)} all-to-all(bf16[4,32,1024]{2,1,0:T(8,128)(2,1)S(1)} %broadcast_in_dim.6), channel_id=1, replica_groups=mesh['fs'=16,'rep'=4,'tp'=2] {'rep'}, dimensions={0} | all-to-all | bytes 524288 | tf_op jit(solution)/shard_map/all_to_all | solution.py:48
  129.7 3.4 %all-to-all-start.2 = ((bf16[4,32,1024]{2,1,0:T(8,128)(2,1)}), bf16[4,32,1024]{2,1,0:T(8,128)(2,1)S(1)}, u32[]{:S(2)}, u32[]{:S(2)}) async-start(bf16[4,32,1024]{2,1,0:T(8,128)(2,1)} %broadcast_in_dim.7), calls=%async_computation.2 | async-start | bytes 524288 | tf_op jit(solution)/shard_map/all_to_all | solution.py:48
  133.4 1.3 multiply_reduce_fusion.1
  134.8 5.0 %all-to-all-done.2 = bf16[4,32,1024]{2,1,0:T(8,128)(2,1)S(1)} async-done(((bf16[4,32,1024]{2,1,0:T(8,128)(2,1)}), bf16[4,32,1024]{2,1,0:T(8,128)(2,1)S(1)}, u32[]{:S(2)}, u32[]{:S(2)}) %all-to-all-start.2) | async-done | bytes 262176 | tf_op jit(solution)/shard_map/all_to_all | solution.py:48
  141.9 1.4 pad_maximum_fusion.4
  143.9 3.8 %all-to-all-start.3 = ((f32[32,1,2]{2,1,0:T(1,128)}), f32[32,1,2]{2,1,0:T(1,128)S(1)}, u32[]{:S(2)}, u32[]{:S(2)}) async-start(f32[32,1,2]{2,1,0:T(1,128)} %broadcast_in_dim.8), calls=%async_computation.3 | async-start | bytes 32768 | tf_op jit(solution)/shard_map/all_to_all | solution.py:48
  148.2 6.8 %all-to-all-done.3 = f32[32,1,2]{2,1,0:T(1,128)S(1)} async-done(((f32[32,1,2]{2,1,0:T(1,128)}), f32[32,1,2]{2,1,0:T(1,128)S(1)}, u32[]{:S(2)}, u32[]{:S(2)}) %all-to-all-start.3) | async-done | bytes 288 | tf_op jit(solution)/shard_map/all_to_all | solution.py:48
  157.0 25.7 %all-gather.6.cloned.1.call-done = bf16[512,2048]{1,0:T(8,128)(2,1)} async-done(((bf16[32,2048]{1,0:T(8,128)(2,1)}), bf16[512,2048]{1,0:T(8,128)(2,1)}) %all-gather.6.cloned.1.call-update) | async-done | bytes 2097168 | tf_op jit(solution)/shard_map/all_gather | solution.py:22
  182.7 1.7 subtract_convert_fusion.4
  184.4 1.7 subtract_convert_fusion.5
  189.0 74.8 %all-gather.8.cloned.1.call-done = bf16[2048,2048]{0,1:T(8,128)(2,1)} async-done(((bf16[128,2048]{0,1:T(8,128)(2,1)}), bf16[2048,2048]{0,1:T(8,128)(2,1)}) %all-gather.8.cloned.1.call-update) | async-done | bytes 8388624 | tf_op jit(solution)/shard_map/all_gather | solution.py:22
  263.8 6.2 %fusion.28 = (bf16[2048,1024]{0,1:T(8,128)(2,1)}, bf16[2048,1024]{0,1:T(8,128)(2,1)}) fusion(bf16[2048,2048]{0,1:T(8,128)(2,1)} %all-gather.8.cloned.1.call-done), kind=kLoop, calls=%fused_computation.41 | loop fusion | bytes 16777216 | tf_op jit(solution)/shard_map/split | solution.py:22
  269.9 6.4 %copy.37 = bf16[2048,1024]{1,0:T(8,128)(2,1)} copy(bf16[2048,1024]{0,1:T(8,128)(2,1)} %get-tuple-element.40) | data formatting | bytes 8388608
  276.3 6.5 %copy.36 = bf16[2048,1024]{1,0:T(8,128)(2,1)} copy(bf16[2048,1024]{0,1:T(8,128)(2,1)} %get-tuple-element.41) | data formatting | bytes 8388608
  (51 shorter events, 8.2 us)
Async XLA Ops:
  7.2 64.0 %copy-start = (bf16[1536,1024]{1,0:T(8,128)(2,1)S(1)}, bf16[1536,1024]{1,0:T(8,128)(2,1)}, u32[]{:S(2)}) copy-start(bf16[1536,1024]{1,0:T(8,128)(2,1)} %param.12) | copy-start | bytes 9437188
  7.2 57.6 %all-gather.4.cloned.1.call-start = ((), (), s32[]{:S(2)}) async-start(), calls=%async_computation.4 | async-start | bytes 4456448 | tf_op jit(solution)/shard_map/all_gather | solution.py:22
  64.7 10.1 %slice-start = ((s8[6291456]{0:T(1024)(128)(4,1)}), s8[4194304]{0:T(1024)(128)(4,1)S(1)}, s32[]{:S(2)}) async-start(s8[6291456]{0:T(1024)(128)(4,1)} %bitcast.22), calls=%async_computation.7 | async-start | bytes 8388608
  71.2 3.7 %slice-start.1 = ((s8[6291456]{0:T(1024)(128)(4,1)}), s8[2097152]{0:T(1024)(128)(4,1)S(1)}, s32[]{:S(2)}) async-start(s8[6291456]{0:T(1024)(128)(4,1)} %bitcast.22), calls=%async_computation.8 | async-start | bytes 4194304
  73.0 2.2 copy-start.10
  75.2 3.5 %copy-start.11 = (bf16[1536,1024]{1,0:T(8,128)(2,1)S(1)}, bf16[1536,1024]{1,0:T(8,128)(2,1)}, u32[]{:S(2)}) copy-start(bf16[1536,1024]{1,0:T(8,128)(2,1)} %param.13) | copy-start | bytes 9437188
  116.0 17.4 %copy-start.6 = (f32[32,1024]{1,0:T(8,128)S(1)}, f32[32,1024]{1,0:T(8,128)}, u32[]{:S(2)}) copy-start(f32[32,1024]{1,0:T(8,128)} %param.18) | copy-start | bytes 393220
  116.0 17.4 %copy-start.7 = (f32[32,1024]{1,0:T(8,128)S(1)}, f32[32,1024]{1,0:T(8,128)}, u32[]{:S(2)}) copy-start(f32[32,1024]{1,0:T(8,128)} %param.16) | copy-start | bytes 393220
  116.0 23.8 %copy-start.8 = (f32[32,1024]{1,0:T(8,128)S(1)}, f32[32,1024]{1,0:T(8,128)}, u32[]{:S(2)}) copy-start(f32[32,1024]{1,0:T(8,128)} %param.19) | copy-start | bytes 393220
  116.0 23.9 %copy-start.9 = (f32[32,1024]{1,0:T(8,128)S(1)}, f32[32,1024]{1,0:T(8,128)}, u32[]{:S(2)}) copy-start(f32[32,1024]{1,0:T(8,128)} %param.17) | copy-start | bytes 393220
  116.0 31.8 %copy-start.2 = (f32[128,1024]{1,0:T(8,128)S(1)}, f32[128,1024]{1,0:T(8,128)}, u32[]{:S(2)}) copy-start(f32[128,1024]{1,0:T(8,128)} %param.20) | copy-start | bytes 1572868
  118.1 29.9 %copy-start.3 = (f32[128,1024]{1,0:T(8,128)S(1)}, f32[128,1024]{1,0:T(8,128)}, u32[]{:S(2)}) copy-start(f32[128,1024]{1,0:T(8,128)} %param.21) | copy-start | bytes 1572868
  118.1 64.6 %copy-start.4 = (bf16[128,512]{1,0:T(8,128)(2,1)S(1)}, bf16[128,512]{1,0:T(8,128)(2,1)}, u32[]{:S(2)}) copy-start(bf16[128,512]{1,0:T(8,128)(2,1)} %param.15) | copy-start | bytes 393220
  129.7 10.1 %all-to-all-start.2 = ((bf16[4,32,1024]{2,1,0:T(8,128)(2,1)}), bf16[4,32,1024]{2,1,0:T(8,128)(2,1)S(1)}, u32[]{:S(2)}, u32[]{:S(2)}) async-start(bf16[4,32,1024]{2,1,0:T(8,128)(2,1)} %broadcast_in_dim.7), calls=%async_computation.2 | async-start | bytes 524288 | tf_op jit(solution)/shard_map/all_to_all | solution.py:48
  133.1 49.6 %all-gather.6.cloned.1.call-start = ((), (), s32[]{:S(2)}) async-start(), calls=%async_computation.5 | async-start | bytes 2228224 | tf_op jit(solution)/shard_map/all_gather | solution.py:22
  134.8 49.7 %copy-start.5 = (bf16[128,512]{1,0:T(8,128)(2,1)S(1)}, bf16[128,512]{1,0:T(8,128)(2,1)}, u32[]{:S(2)}) copy-start(bf16[128,512]{1,0:T(8,128)(2,1)} %param.14) | copy-start | bytes 393220
  143.9 11.1 %all-to-all-start.3 = ((f32[32,1,2]{2,1,0:T(1,128)}), f32[32,1,2]{2,1,0:T(1,128)S(1)}, u32[]{:S(2)}, u32[]{:S(2)}) async-start(f32[32,1,2]{2,1,0:T(1,128)} %broadcast_in_dim.8), calls=%async_computation.3 | async-start | bytes 32768 | tf_op jit(solution)/shard_map/all_to_all | solution.py:48
  147.7 116.1 %all-gather.8.cloned.1.call-start = ((), (), s32[]{:S(2)}) async-start(), calls=%async_computation.6 | async-start | bytes 8912896 | tf_op jit(solution)/shard_map/all_gather | solution.py:22
  276.3 6.5 %copy-start.1 = (bf16[1536,1024]{1,0:T(8,128)(2,1)S(1)}, bf16[1536,1024]{1,0:T(8,128)(2,1)}, u32[]{:S(2)}) copy-start(bf16[1536,1024]{1,0:T(8,128)(2,1)} %param.12) | copy-start | bytes 9437188
Sparse Core Ops, SparseCore 0:
  10.7 53.9 all-gather.3
  142.0 40.6 all-gather.5
  187.1 76.5 all-gather.7
where the time goes:
time: 290 us; the launch traced here: 289 us
  waiting for transfers between devices  168 us (58%)
  blocking collectives  44.3 us (15%)
  local copies, waits for them, and re-layouts  23.8 us (8%)
  matrix products  20.6 us (7%)
  between operations  15.4 us (5%)
  other arithmetic  9.77 us (3%)
  starting transfers between devices  7.54 us (3%)
    all_gather x3, waiting for transfers between devices, in_one_piece(): lax.all_gather(both, axis, axis=dim, tiled=True)  156 us
    all_to_all x1, blocking collectives, summed_on_arrival(): tiles = lax.all_to_all(in_blocks(x, dim, size), axis, 0, 0, tiled=True)  33.4 us
    unnamed x34, local copies, waits for them, and re-layouts  15.7 us
    all_to_all x2, waiting for transfers between devices, sent_to_all(): lax.all_to_all(jnp.broadcast_to(x[None], (size, *x.shape)), axis, 0, 0, t...  11.8 us
    all_to_all x1, blocking collectives, sent_to_all(): lax.all_to_all(jnp.broadcast_to(x[None], (size, *x.shape)), axis, 0, 0, t...  10.9 us
    all_to_all x2, starting transfers between devices, sent_to_all(): lax.all_to_all(jnp.broadcast_to(x[None], (size, *x.shape)), axis, 0, 0, t...  7.24 us
    dot_general x1, matrix products, body(): proj_rec = jnp.dot(normed_in, pieces[0], preferred_element_type=jnp.float32)  6.4 us
    split x1, local copies, waits for them, and re-layouts, in_one_piece(): jnp.split(lax.all_gather(both, axis, axis=dim, tiled=True), ends, axis=al...  6.15 us
  transfers between devices with their start and end apart: 5, of which 5 were waited for; matrix products, arithmetic and copies ran while one was open for 2% of the time, Pallas kernels for 0%

commit v1 on v0

v1 whole, which is shorter than its diff:
```python
import jax
import jax.numpy as jnp
from jax import lax
from jax.experimental import pallas as pl
from jax.experimental.pallas import tpu as pltpu
from jax.sharding import PartitionSpec as P

MESH = pl.DeviceIdType.MESH
BF = jnp.bfloat16
F32 = jnp.float32

D = 2048
DR = 2048
RANK = 512
ENTRIES = float(RANK * DR)
TOK = 1536
HALF = 1024

beta_first = 0.8
beta_second = 0.9
scale_floor = 0.25
step_rate = 0.01

GATHER_ORDER = (("x", "y", "z"), ("y", "z", "x"), ("z", "x", "y"))
COLS = ((0, 384), (384, 384), (768, 256))
SPLIT = (256, 128, 128)
WIDE_COLS = ((0, 640), (640, 640), (1280, 768))
N_SEMS = 172


def ring_kernel(
    normed_ref,
    cot_rec_ref,
    cot_gate_ref,
    fac_rec_ref,
    fac_gate_ref,
    first_rec_ref,
    first_gate_ref,
    second_rec_ref,
    second_gate_ref,
    master_rec_ref,
    master_gate_ref,
    fac,
    direc,
    mast,
    lowx,
    sq,
    xs,
    cots,
    proj_t,
    part,
    moms,
    mast_f,
    low,
    sq_own,
    sq_other,
    lefts,
    left_ones,
    rights,
    right_ones,
    send_sems,
    recv_sems,
    local_sems,
):
    f, x, c = lax.axis_index("fs"), lax.axis_index("rep"), lax.axis_index("tp")
    me = {"x": x, "y": lax.rem(f, 4), "z": lax.div(f, 4)}
    count = [0]
    started = []

    def coord(dim, delta):
        return lax.rem(me[dim] + (delta + 4) % 4, 4)

    def device(dim, delta):
        if dim == "core":
            return {"tp": 1 - c}
        p = coord(dim, delta)
        if dim == "x":
            return {"rep": p}
        if dim == "y":
            return {"fs": me["z"] * 4 + p}
        return {"fs": p * 4 + me["y"]}

    def send(src, dst, dim, delta):
        k = count[0]
        count[0] += 1
        copy = pltpu.make_async_remote_copy(
            src_ref=src,
            dst_ref=dst,
            send_sem=send_sems.at[k],
            recv_sem=recv_sems.at[k],
            device_id=device(dim, delta),
            device_id_type=MESH,
        )
        copy.start()
        started.append(copy)
        return copy

    def full(v):
        return slice(None) if v is None else v

    def rank_index(at):
        xx = at["x"]
        if xx is None:
            return (slice(None), full(at["z"]), full(at["y"]), slice(None))
        return (lax.div(xx, 2), full(at["z"]), full(at["y"]), lax.rem(xx, 2))

    def fac_index(at):
        return (full(at["z"]), full(at["y"]), full(at["x"]), c)

    def mast_index(at):
        return (full(at["z"]), full(at["y"]), full(at["x"]))

    def col_parts(s):
        base, width = COLS[s]
        one = SPLIT[s]
        rows = slice(None)
        return (
            (rows, pl.ds(base, width)),
            (rows, pl.ds(base, one)),
            (rows, pl.ds(base + one, width - one)),
        )

    def row_parts(s):
        base, width = WIDE_COLS[s]
        cols = pl.ds(base, width)
        return ((slice(None), cols), (pl.ds(0, 16), cols), (pl.ds(16, 16), cols))

    def gather(buf, index, parts):
        for k in range(3):
            sent = []
            for s in range(3):
                order = GATHER_ORDER[s]
                at = {d: (None if d in order[:k] else me[d]) for d in order}
                whole, _, _ = parts(s)
                view = buf.at[index(at) + whole]
                sent.append(
                    (send(view, view, order[k], 1), send(view, view, order[k], -1))
                )
            yield
            passed = []
            for s in range(3):
                order = GATHER_ORDER[s]
                _, one, two = parts(s)
                at = {d: (None if d in order[:k] else me[d]) for d in order}
                sent[s][0].wait_recv()
                at[order[k]] = coord(order[k], -1)
                view = buf.at[index(at) + one]
                a = send(view, view, order[k], 1)
                sent[s][1].wait_recv()
                at[order[k]] = coord(order[k], 1)
                view = buf.at[index(at) + two]
                b = send(view, view, order[k], -1)
                passed.append((a, b))
            yield
            for a, b in passed:
                a.wait_recv()
                b.wait_recv()
        yield

    local = []

    def fetch(src, dst):
        copy = pltpu.make_async_copy(src, dst, local_sems.at[len(local)])
        copy.start()
        local.append(copy)
        return copy

    own_rows = pl.ds(pl.multiple_of((2 * x + c) * 16, 16), 16)
    own_fac = fac_index(me)
    fac_in = [
        fetch(r.at[own_rows], fac.at[own_fac + (slice(None), pl.ds(512 * m, 512))])
        for m, r in enumerate((fac_rec_ref, fac_gate_ref))
    ]
    quarter = pl.ds(pl.multiple_of(x * 32, 32), 32)
    mast_in = [
        fetch(r.at[quarter], mast_f.at[m])
        for m, r in enumerate((master_rec_ref, master_gate_ref))
    ]
    x_in = [
        fetch(normed_ref.at[pl.ds(256 * i, 256)], xs.at[i]) for i in range(6)
    ]
    cot_in = [fetch(r, cots.at[m]) for m, r in enumerate((cot_rec_ref, cot_gate_ref))]
    mom_in = [
        fetch(r, moms.at[i])
        for i, r in enumerate(
            (first_rec_ref, first_gate_ref, second_rec_ref, second_gate_ref)
        )
    ]

    barrier = pltpu.get_barrier_semaphore()
    for dim, delta in (("x", 1), ("x", -1), ("y", 1), ("y", -1), ("z", 1), ("z", -1), ("core", 0)):
        pl.semaphore_signal(
            barrier, inc=1, device_id=device(dim, delta), device_id_type=MESH
        )
    for copy in mast_in:
        copy.wait()
    own_mast = mast_index(me)
    for m in range(2):
        mast[own_mast + (slice(None), pl.ds(1024 * m, 1024))] = mast_f[m].astype(BF)
    for copy in fac_in:
        copy.wait()
    pl.semaphore_wait(barrier, 7)

    facs = gather(fac, fac_index, col_parts)
    masts = gather(mast, mast_index, row_parts)
    for _ in range(2):
        next(facs)
        next(masts)
    for _ in range(4):
        next(facs)
    next(masts)
    next(facs)
    swap = []
    for s in range(3):
        whole = col_parts(s)[0]
        view = fac.at[(slice(None), slice(None), slice(None), c) + whole]
        swap.append(send(view, view, "core", 0))
    next(masts)
    for copy in swap:
        copy.wait_recv()
    for copy in x_in:
        copy.wait()

    def project(lo, hi):
        def one(i, carry):
            tokens = pl.ds(pl.multiple_of(i * 256, 256), 256)
            for m in range(2):
                cols = pl.ds(512 * m, 512)
                factor = fac[:, :, :, :, :, cols].reshape(D, 512)
                got = jnp.dot(xs[i], factor, preferred_element_type=F32)
                proj_t[m, :, tokens] = got.astype(BF).T
            return carry

        lax.fori_loop(lo, hi, one, 0)

    project(0, 3)
    next(masts)
    project(3, 6)
    for copy in cot_in:
        copy.wait()

    for m in range(2):

        def one(j, carry):
            cols = pl.ds(pl.multiple_of(j * 512, 512), 512)
            got = jnp.dot(proj_t[m], cots[m, :, cols], preferred_element_type=F32)
            part[m, :, :, :, :, cols] = got.astype(BF).reshape(4, 4, 2, 16, 512)
            return carry

        lax.fori_loop(0, 2, one, 0)

    for k in range(3):
        sent = []
        views = []
        for s in range(3):
            order = GATHER_ORDER[s][::-1]
            e = order[k]
            whole, one, two = col_parts(s)
            width, half = COLS[s][1], SPLIT[s]

            def group(delta, cut, e=e, order=order, k=k):
                at = {d: (me[d] if d in order[:k] else None) for d in order}
                at[e] = coord(e, delta)
                return part.at[rank_index(at) + cut]

            left, left_one = lefts[3 * s + k], left_ones[3 * s + k]
            right, right_one = rights[3 * s + k], right_ones[3 * s + k]
            lead = (slice(None),) * (len(left.shape) - 1)
            left_a = left.at[lead + (pl.ds(0, half),)]
            left_b = left.at[lead + (pl.ds(half, width - half),)]
            right_a = right.at[lead + (pl.ds(0, half),)]
            right_b = right.at[lead + (pl.ds(half, width - half),)]
            sent.append(
                [
                    send(group(2, one), left_one, e, 1),
                    send(group(2, two), right_one, e, -1),
                    send(group(1, two), left_b, e, 1),
                    send(group(-1, one), right_a, e, -1),
                ]
            )
            views.append((group, e, one, two, whole, left_one, right_one, left_a, right_b, left, right))
        for s in range(3):
            group, e, one, two, whole, left_one, right_one, left_a, right_b, left, right = views[s]
            sent[s][0].wait_recv()
            v = group(1, one)
            v[...] = (v[...].astype(F32) + left_one[...].astype(F32)).astype(BF)
            sent[s].append(send(v, left_a, e, 1))
            sent[s][1].wait_recv()
            v = group(-1, two)
            v[...] = (v[...].astype(F32) + right_one[...].astype(F32)).astype(BF)
            sent[s].append(send(v, right_b, e, -1))
        for s in range(3):
            group, e, one, two, whole, left_one, right_one, left_a, right_b, left, right = views[s]
            for copy in sent[s][2:]:
                copy.wait_recv()
            v = group(0, whole)
            total = (
                v[...].astype(F32) + left[...].astype(F32) + right[...].astype(F32)
            )
            if k < 2:
                v[...] = total.astype(BF)
            else:
                low[whole] = total

    for copy in mom_in:
        copy.wait()
    m, h = lax.div(x, 2), lax.rem(x, 2)
    rows = pl.ds(pl.multiple_of(h * 16, 16), 16)
    got = low[...]
    lowx[m, h] = got.astype(BF)
    new_first = beta_first * moms[m, rows] + (1.0 - beta_first) * got
    new_second = beta_second * moms[2 + m, rows] + (1.0 - beta_second) * got * got
    direc[rank_index(me)] = (new_first / jnp.sqrt(new_second)).astype(BF)

    direcs = gather(direc, rank_index, col_parts)
    next(direcs)
    low_view = lowx.at[m, h]
    low_sent = (send(low_view, low_view, "x", 1), send(low_view, low_view, "x", -1))
    next(direcs)
    next(direcs)
    low_sent[0].wait_recv()
    xl = coord("x", -1)
    view = lowx.at[lax.div(xl, 2), lax.rem(xl, 2), :, pl.ds(0, 512)]
    low_a = send(view, view, "x", 1)
    low_sent[1].wait_recv()
    xr = coord("x", 1)
    view = lowx.at[lax.div(xr, 2), lax.rem(xr, 2), :, pl.ds(512, 512)]
    low_b = send(view, view, "x", -1)
    next(direcs)
    next(direcs)
    next(direcs)
    next(masts)
    next(direcs)

    for m in range(2):

        def add(z, acc):
            v = direc[m, z].astype(F32)
            v = jnp.sum((v * v).reshape(16, 8, 1024), axis=0)
            for j in range(8):
                acc = acc + v[:, 128 * j : 128 * (j + 1)]
            return acc

        sq_own[m] = lax.fori_loop(0, 4, add, jnp.zeros((8, 128), F32))
    swapped = send(sq_own, sq_other, "core", 0)
    low_a.wait_recv()
    low_b.wait_recv()
    next(masts)
    swapped.wait_recv()
    sq[...] = sq_own[...] + sq_other[...]
    for copy in started:
        copy.wait_send()


def update_kernel(
    fac,
    direc,
    mast,
    lowx,
    sq,
    first_rec,
    first_gate,
    second_rec,
    second_gate,
    upd_rec,
    upd_gate,
    nf_rec,
    nf_gate,
    ns_rec,
    ns_gate,
    copy_rec,
    copy_gate,
):
    i = pl.program_id(0)
    f = lax.axis_index("fs")

    def scale_of(m):
        total = jnp.sum(sq[m], keepdims=True)
        return 1.0 / jnp.sqrt(total / ENTRIES + scale_floor)

    scales = [scale_of(m) for m in range(2)]

    @pl.when(i == 0)
    def _():
        own = pl.ds(pl.multiple_of(f * 128, 128), 128)
        for m, (upd, nf, ns, first, second) in enumerate(
            (
                (upd_rec, nf_rec, ns_rec, first_rec, second_rec),
                (upd_gate, nf_gate, ns_gate, first_gate, second_gate),
            )
        ):
            got = jnp.dot(
                fac[own, 512 * m : 512 * (m + 1)],
                direc[m],
                preferred_element_type=F32,
            )
            upd[...] = got * scales[m]
            low = lowx[m].astype(F32)
            nf[...] = beta_first * first[...] + (1.0 - beta_first) * low
            ns[...] = beta_second * second[...] + (1.0 - beta_second) * low * low

    rows = pl.ds(pl.multiple_of(i * 256, 256), 256)
    for m, out in enumerate((copy_rec, copy_gate)):
        got = jnp.dot(
            fac[rows, 512 * m : 512 * (m + 1)], direc[m], preferred_element_type=F32
        )
        upd = got * scales[m]
        old = mast[rows, 1024 * m : 1024 * (m + 1)].astype(F32)
        out[...] = (old - step_rate * upd).astype(BF)


def recv_shapes(extra):
    dims = {"x": (2, 2), "y": 4, "z": 4}
    out = []
    for s in range(3):
        order = GATHER_ORDER[s][::-1]
        for k in range(3):
            free = order[k + 1 :]
            lead = []
            if "x" in free:
                lead.append(2)
            if "z" in free:
                lead.append(4)
            if "y" in free:
                lead.append(4)
            if "x" in free:
                lead.append(2)
            width = {
                "all": COLS[s][1],
                "one": SPLIT[s],
                "two": COLS[s][1] - SPLIT[s],
            }[extra]
            out.append(pltpu.VMEM((*lead, 16, width), BF))
    return out


def body(
    normed_in,
    cotan_rec,
    cotan_gate,
    factor_rec,
    factor_gate,
    first_rec,
    first_gate,
    second_rec,
    second_gate,
    master_rec,
    master_gate,
):
    hbm = pl.BlockSpec(memory_space=pl.ANY)
    vmem = pl.BlockSpec(memory_space=pltpu.VMEM)
    fac, direc, mast, lowx, sq = pl.pallas_call(
        ring_kernel,
        name="rings",
        out_shape=(
            jax.ShapeDtypeStruct((4, 4, 4, 2, 16, 1024), BF),
            jax.ShapeDtypeStruct((2, 4, 4, 2, 16, 1024), BF),
            jax.ShapeDtypeStruct((4, 4, 4, 32, 2048), BF),
            jax.ShapeDtypeStruct((2, 2, 16, 1024), BF),
            jax.ShapeDtypeStruct((2, 8, 128), F32),
        ),
        in_specs=[hbm] * 11,
        out_specs=(vmem,) * 5,
        scratch_shapes=[
            pltpu.VMEM((6, 256, D), BF),
            pltpu.VMEM((2, TOK, HALF), BF),
            pltpu.VMEM((2, RANK, TOK), BF),
            pltpu.VMEM((2, 4, 4, 2, 16, 1024), BF),
            pltpu.VMEM((4, 32, 1024), F32),
            pltpu.VMEM((2, 32, 1024), F32),
            pltpu.VMEM((16, 1024), F32),
            pltpu.VMEM((2, 8, 128), F32),
            pltpu.VMEM((2, 8, 128), F32),
            recv_shapes("all"),
            recv_shapes("one"),
            recv_shapes("all"),
            recv_shapes("two"),
            pltpu.SemaphoreType.DMA((N_SEMS,)),
            pltpu.SemaphoreType.DMA((N_SEMS,)),
            pltpu.SemaphoreType.DMA((16,)),
        ],
        compiler_params=pltpu.CompilerParams(
            collective_id=0, has_side_effects=True, vmem_limit_bytes=52 << 20
        ),
    )(
        normed_in,
        cotan_rec,
        cotan_gate,
        factor_rec,
        factor_gate,
        first_rec,
        first_gate,
        second_rec,
        second_gate,
        master_rec,
        master_gate,
    )
    fac = fac.reshape(D, 2 * RANK)
    direc = direc.reshape(2, RANK, HALF)
    mast = mast.reshape(D, 2 * HALF)
    lowx = lowx.reshape(2, 32, HALF)

    def once(shape):
        return pl.BlockSpec(shape, lambda i: (0,) * len(shape))

    row = pl.BlockSpec((256, HALF), lambda i: (i, 0))
    return pl.pallas_call(
        update_kernel,
        name="update",
        grid=(8,),
        out_shape=(
            *(jax.ShapeDtypeStruct((128, HALF), F32),) * 2,
            *(jax.ShapeDtypeStruct((32, HALF), F32),) * 4,
            *(jax.ShapeDtypeStruct((D, HALF), BF),) * 2,
        ),
        in_specs=[vmem] * 9,
        out_specs=(*(once((128, HALF)),) * 2, *(once((32, HALF)),) * 4, row, row),
        compiler_params=pltpu.CompilerParams(vmem_limit_bytes=48 << 20),
    )(fac, direc, mast, lowx, sq, first_rec, first_gate, second_rec, second_gate)


def solution(mesh):
    return jax.shard_map(
        body,
        mesh=mesh,
        in_specs=(
            P(("fs", "rep"), None),
            P(("fs", "rep"), "tp"),
            P(("fs", "rep"), "tp"),
            P("fs", None),
            P("fs", None),
            P("fs", "tp"),
            P("fs", "tp"),
            P("fs", "tp"),
            P("fs", "tp"),
            P("fs", "tp"),
            P("fs", "tp"),
        ),
        out_specs=(
            P("fs", "tp"),
            P("fs", "tp"),
            P("fs", "tp"),
            P("fs", "tp"),
            P("fs", "tp"),
            P("fs", "tp"),
            P(None, "tp"),
            P(None, "tp"),
        ),
        check_vma=False,
    )
```

time: 290 us -> 140 us (0.48)
  waiting for transfers between devices: 168 us -> 0 us
  Pallas kernels: 0 us -> 130 us
  blocking collectives: 44.3 us -> 0 us
  matrix products: 20.6 us -> 0 us
  between operations: 15.4 us -> 0.67 us
  local copies, waits for them, and re-layouts: 23.8 us -> 9.08 us
  other arithmetic: 9.77 us -> 0 us
  starting transfers between devices: 7.54 us -> 0 us
    all_gather x3 -> x0, waiting for transfers between devices: 156 us -> none  [in_one_piece(): lax.all_gather(both, axis, axis=dim, tiled=True)]
    pallas_call x0 -> x2, Pallas kernels: none -> 130 us  [the longest x1 116 us: body(): pl.pallas_call(ring_kernel, name='rings', out_shape=(jax.ShapeDtypeStruct...]
    all_to_all x2 -> x0, blocking collectives: 44.3 us -> none  [the longest x1 33.4 us: summed_on_arrival(): tiles = lax.all_to_all(in_blocks(x, dim, size), axis, 0, 0, tiled=True)]
    dot_general x8 -> x0, matrix products: 20.6 us -> none  [the longest x1 6.4 us: body(): proj_rec = jnp.dot(normed_in, pieces[0], preferred_element_type=jnp.float32)]
    all_to_all x2 -> x0, waiting for transfers between devices: 11.8 us -> none  [sent_to_all(): lax.all_to_all(jnp.broadcast_to(x[None], (size, *x.shape)), axis, 0, 0, t...]
    all_to_all x2 -> x0, starting transfers between devices: 7.24 us -> none  [sent_to_all(): lax.all_to_all(jnp.broadcast_to(x[None], (size, *x.shape)), axis, 0, 0, t...]
    unnamed x34 -> x18, local copies, waits for them, and re-layouts: 15.7 us -> 9.08 us
    split x1 -> x0, local copies, waits for them, and re-layouts: 6.15 us -> none  [in_one_piece(): jnp.split(lax.all_gather(both, axis, axis=dim, tiled=True), ends, axis=al...]
  transfers between devices with their start and end apart: 5 -> 0, of which waited for: 5 -> 0; matrix products, arithmetic and copies ran while one was open for 2% -> 0% of each run, Pallas kernels for 0% -> 0%
where the time goes in v1:
time: 140 us; the launch traced here: 139 us
  Pallas kernels  130 us (93%)
  local copies, waits for them, and re-layouts  9.08 us (6%)
    pallas_call x1, Pallas kernels, body(): pl.pallas_call(ring_kernel, name='rings', out_shape=(jax.ShapeDtypeStruct...  116 us
    pallas_call x1, Pallas kernels, body(): pl.pallas_call(update_kernel, name='update', grid=(8,), out_shape=(*(jax....  13.5 us
    unnamed x18, local copies, waits for them, and re-layouts  9.08 us

profile of v1, /device:TPU:0, one launch (start us, length us, event | category | flops | bytes accessed | tf_op | source)
XLA Modules:
  0.0 139.3 jit_solution(7685261071191072291)
XLA Ops:
  0.6 0.0 copy-start.1
  0.6 0.9 copy-done.1
  1.5 0.0 copy-start.2
  1.5 0.9 copy-done.2
  2.4 0.0 copy-start.3
  2.4 0.9 copy-done.3
  3.4 0.0 copy-start.4
  3.4 0.9 copy-done.4
  4.3 0.0 copy-start.5
  4.3 1.0 copy-done.5
  5.3 0.0 copy-start.6
  5.3 1.0 copy-done.6
  6.3 0.0 copy-start.7
  6.3 0.9 copy-done.7
  7.2 0.0 copy-start.8
  7.2 0.9 copy-done.8
  8.2 116.0 %rings.1 = (bf16[4,4,4,2,16,1024]{5,4,3,2,1,0:T(8,128)(2,1)}, bf16[2,4,4,2,16,1024]{5,4,3,2,1,0:T(8,128)(2,1)}, bf16[4,4,4,32,2048]{4,3,2,1,0:T(8,128)(2,1)}, bf...) custom-call(bf16[1536,2048]{1,0:T(8,128)(2,1)} %normed_ref.1, bf16[1536,1024]{1,0:T(8,128)(2,1)} %cot_rec_ref.1, ...), custom_call_target="tpu_custom_call" | custom-call | tf_op jit(solution)/shard_map/rings/pallas_call | solution.py:452
  124.2 0.0 copy-start
  124.2 1.6 %copy-done = bf16[2,4,4,2,16,1024]{5,4,3,2,1,0:T(8,128)(2,1)S(1)} copy-done((bf16[2,4,4,2,16,1024]{5,4,3,2,1,0:T(8,128)(2,1)S(1)}, bf16[2,4,4,2,16,1024]{5,4,3,2,1,0:T(8,128)(2,1)}, u32[]{:S(2)}) %copy-start) | copy-done | bytes 2097176
  125.8 13.5 %update.1 = (f32[128,1024]{1,0:T(8,128)}, f32[128,1024]{1,0:T(8,128)}, f32[32,1024]{1,0:T(8,128)}, f32[32,1024]{1,0:T(8,128)}, f32[32,1024]{1,0:T(8,128)}, /*ind...) custom-call(bf16[2048,1024]{1,0:T(8,128)(2,1)} %bitcast.7, ...), custom_call_target="tpu_custom_call" | custom-call | tf_op jit(solution)/shard_map/update/pallas_call | solution.py:507
Async XLA Ops:
  0.6 0.9 copy-start.1
  1.5 0.9 copy-start.2
  2.4 0.9 copy-start.3
  3.4 0.9 copy-start.4
  4.3 1.0 copy-start.5
  5.3 1.0 copy-start.6
  6.3 0.9 copy-start.7
  7.2 0.9 copy-start.8
  124.2 1.6 %copy-start = (bf16[2,4,4,2,16,1024]{5,4,3,2,1,0:T(8,128)(2,1)S(1)}, bf16[2,4,4,2,16,1024]{5,4,3,2,1,0:T(8,128)(2,1)}, u32[]{:S(2)}) copy-start(bf16[2,4,4,2,16,1024]{5,4,3,2,1,0:T(8,128)(2,1)} %get-tuple-element.14) | copy-start | bytes 6291460

commit v2 on v1

--- a/solution.py
+++ b/solution.py
@@ -199,27 +199,35 @@
         mast[own_mast + (slice(None), pl.ds(1024 * m, 1024))] = mast_f[m].astype(BF)
     for copy in fac_in:
         copy.wait()
-    pl.semaphore_wait(barrier, 7)
+    with jax.named_scope("barrier"):
+        pl.semaphore_wait(barrier, 7)
 
     facs = gather(fac, fac_index, col_parts)
     masts = gather(mast, mast_index, row_parts)
-    for _ in range(2):
-        next(facs)
-        next(masts)
-    for _ in range(4):
-        next(facs)
-    next(masts)
-    next(facs)
+
+    def step(it, name):
+        with jax.named_scope(name):
+            next(it)
+
+    for i in range(2):
+        step(facs, f"fac{i}")
+        step(masts, f"mast{i}")
+    for i in range(2, 6):
+        step(facs, f"fac{i}")
+    step(masts, "mast2")
+    step(facs, "fac6")
     swap = []
     for s in range(3):
         whole = col_parts(s)[0]
         view = fac.at[(slice(None), slice(None), slice(None), c) + whole]
         swap.append(send(view, view, "core", 0))
-    next(masts)
-    for copy in swap:
-        copy.wait_recv()
-    for copy in x_in:
-        copy.wait()
+    step(masts, "mast3")
+    with jax.named_scope("swap"):
+        for copy in swap:
+            copy.wait_recv()
+    with jax.named_scope("xin"):
+        for copy in x_in:
+            copy.wait()
 
     def project(lo, hi):
         def one(i, carry):
@@ -233,9 +241,11 @@
 
         lax.fori_loop(lo, hi, one, 0)
 
-    project(0, 3)
-    next(masts)
-    project(3, 6)
+    with jax.named_scope("proj0"):
+        project(0, 3)
+    step(masts, "mast4")
+    with jax.named_scope("proj1"):
+        project(3, 6)
     for copy in cot_in:
         copy.wait()
 
@@ -247,7 +257,8 @@
             part[m, :, :, :, :, cols] = got.astype(BF).reshape(4, 4, 2, 16, 512)
             return carry
 
-        lax.fori_loop(0, 2, one, 0)
+        with jax.named_scope("part"):
+            lax.fori_loop(0, 2, one, 0)
 
     for k in range(3):
         sent = []
@@ -279,6 +290,8 @@
                 ]
             )
             views.append((group, e, one, two, whole, left_one, right_one, left_a, right_b, left, right))
+        mark = jax.named_scope(f"rs_pass{k}")
+        mark.__enter__()
         for s in range(3):
             group, e, one, two, whole, left_one, right_one, left_a, right_b, left, right = views[s]
             sent[s][0].wait_recv()
@@ -289,6 +302,9 @@
             v = group(-1, two)
             v[...] = (v[...].astype(F32) + right_one[...].astype(F32)).astype(BF)
             sent[s].append(send(v, right_b, e, -1))
+        mark.__exit__(None, None, None)
+        mark = jax.named_scope(f"rs_sum{k}")
+        mark.__enter__()
         for s in range(3):
             group, e, one, two, whole, left_one, right_one, left_a, right_b, left, right = views[s]
             for copy in sent[s][2:]:
@@ -301,6 +317,7 @@
                 v[...] = total.astype(BF)
             else:
                 low[whole] = total
+        mark.__exit__(None, None, None)
 
     for copy in mom_in:
         copy.wait()
@@ -313,11 +330,11 @@
     direc[rank_index(me)] = (new_first / jnp.sqrt(new_second)).astype(BF)
 
     direcs = gather(direc, rank_index, col_parts)
-    next(direcs)
+    step(direcs, "dir0")
     low_view = lowx.at[m, h]
     low_sent = (send(low_view, low_view, "x", 1), send(low_view, low_view, "x", -1))
-    next(direcs)
-    next(direcs)
+    step(direcs, "dir1")
+    step(direcs, "dir2")
     low_sent[0].wait_recv()
     xl = coord("x", -1)
     view = lowx.at[lax.div(xl, 2), lax.rem(xl, 2), :, pl.ds(0, 512)]
@@ -326,11 +343,11 @@
     xr = coord("x", 1)
     view = lowx.at[lax.div(xr, 2), lax.rem(xr, 2), :, pl.ds(512, 512)]
     low_b = send(view, view, "x", -1)
-    next(direcs)
-    next(direcs)
-    next(direcs)
-    next(masts)
-    next(direcs)
+    step(direcs, "dir3")
+    step(direcs, "dir4")
+    step(direcs, "dir5")
+    step(masts, "mast5")
+    step(direcs, "dir6")
 
     for m in range(2):
 
@@ -341,15 +358,17 @@
                 acc = acc + v[:, 128 * j : 128 * (j + 1)]
             return acc
 
-        sq_own[m] = lax.fori_loop(0, 4, add, jnp.zeros((8, 128), F32))
+        with jax.named_scope("squares"):
+            sq_own[m] = lax.fori_loop(0, 4, add, jnp.zeros((8, 128), F32))
     swapped = send(sq_own, sq_other, "core", 0)
     low_a.wait_recv()
     low_b.wait_recv()
-    next(masts)
+    step(masts, "mast6")
     swapped.wait_recv()
     sq[...] = sq_own[...] + sq_other[...]
-    for copy in started:
-        copy.wait_send()
+    with jax.named_scope("drain"):
+        for copy in started:
+            copy.wait_send()
 
 
 def update_kernel(
@@ -447,17 +466,17 @@
     master_rec,
     master_gate,
 ):
-    hbm = pl.BlockSpec(memory_space=pl.ANY)
+    hbm = pl.BlockSpec(memory_space=pltpu.HBM)
     vmem = pl.BlockSpec(memory_space=pltpu.VMEM)
     fac, direc, mast, lowx, sq = pl.pallas_call(
         ring_kernel,
         name="rings",
         out_shape=(
-            jax.ShapeDtypeStruct((4, 4, 4, 2, 16, 1024), BF),
-            jax.ShapeDtypeStruct((2, 4, 4, 2, 16, 1024), BF),
-            jax.ShapeDtypeStruct((4, 4, 4, 32, 2048), BF),
-            jax.ShapeDtypeStruct((2, 2, 16, 1024), BF),
-            jax.ShapeDtypeStruct((2, 8, 128), F32),
+            pltpu.VMEM((4, 4, 4, 2, 16, 1024), BF),
+            pltpu.VMEM((2, 4, 4, 2, 16, 1024), BF),
+            pltpu.VMEM((4, 4, 4, 32, 2048), BF),
+            pltpu.VMEM((2, 2, 16, 1024), BF),
+            pltpu.VMEM((2, 8, 128), F32),
         ),
         in_specs=[hbm] * 11,
         out_specs=(vmem,) * 5,
@@ -480,7 +499,7 @@
             pltpu.SemaphoreType.DMA((16,)),
         ],
         compiler_params=pltpu.CompilerParams(
-            collective_id=0, has_side_effects=True, vmem_limit_bytes=52 << 20
+            collective_id=0, has_side_effects=True, vmem_limit_bytes=40 << 20
         ),
     )(
         normed_in,
@@ -515,7 +534,7 @@
         ),
         in_specs=[vmem] * 9,
         out_specs=(*(once((128, HALF)),) * 2, *(once((32, HALF)),) * 4, row, row),
-        compiler_params=pltpu.CompilerParams(vmem_limit_bytes=48 << 20),
+        compiler_params=pltpu.CompilerParams(vmem_limit_bytes=24 << 20),
     )(fac, direc, mast, lowx, sq, first_rec, first_gate, second_rec, second_gate)
 
 

time: 140 us -> 120 us (0.86)
  Pallas kernels: 130 us -> 119 us
  local copies, waits for them, and re-layouts: 9.08 us -> 0.02 us
    unnamed x18 -> x8, local copies, waits for them, and re-layouts: 9.08 us -> 0.02 us
    pallas_call x1, Pallas kernels: 116 us -> 110 us  [body(): pl.pallas_call(ring_kernel, name='rings', out_shape=(pltpu.VMEM((4, 4, 4,...]
    pallas_call x1, Pallas kernels: 13.5 us -> 8.84 us  [body(): pl.pallas_call(update_kernel, name='update', grid=(8,), out_shape=(*(jax....]
where the time goes in v2:
time: 120 us
  Pallas kernels  119 us (99%)
    pallas_call x1, Pallas kernels, body(): pl.pallas_call(ring_kernel, name='rings', out_shape=(pltpu.VMEM((4, 4, 4,...  110 us
    pallas_call x1, Pallas kernels, body(): pl.pallas_call(update_kernel, name='update', grid=(8,), out_shape=(*(jax....  8.84 us

profile of v2, /device:TPU:0, one launch (start us, length us, event | category | flops | bytes accessed | tf_op | source)
XLA Modules:
  0.0 119.7 jit_solution(13757913069415120987)
XLA Ops:
  0.6 0.0 copy-start.3
  0.6 0.0 copy-start.2
  0.7 0.0 copy-start.1
  0.7 0.0 copy-start
  0.7 110.1 %rings.1 = (bf16[4,4,4,2,16,1024]{5,4,3,2,1,0:T(8,128)(2,1)S(1)}, bf16[2,4,4,2,16,1024]{5,4,3,2,1,0:T(8,128)(2,1)S(1)}, bf16[4,4,4,32,2048]{4,3,2,1,0:T(8,128)(2...) custom-call(bf16[1536,2048]{1,0:T(8,128)(2,1)} %normed_ref.1, bf16[1536,1024]{1,0:T(8,128)(2,1)} %cot_rec_ref.1, ...), custom_call_target="tpu_custom_call" | custom-call | tf_op jit(solution)/shard_map/rings/pallas_call | solution.py:471
  110.8 0.0 copy-done.3
  110.8 0.0 copy-done.2
  110.8 0.0 copy-done.1
  110.8 0.0 copy-done
  110.8 8.8 %update.1 = (f32[128,1024]{1,0:T(8,128)}, f32[128,1024]{1,0:T(8,128)}, f32[32,1024]{1,0:T(8,128)}, f32[32,1024]{1,0:T(8,128)}, f32[32,1024]{1,0:T(8,128)}, /*ind...) custom-call(bf16[2048,1024]{1,0:T(8,128)(2,1)S(1)} %bitcast.5, ...), custom_call_target="tpu_custom_call" | custom-call | tf_op jit(solution)/shard_map/update/pallas_call | solution.py:526
Async XLA Ops:
  0.6 110.2 %copy-start.3 = (f32[32,1024]{1,0:T(8,128)S(1)}, f32[32,1024]{1,0:T(8,128)}, u32[]{:S(2)}) copy-start(f32[32,1024]{1,0:T(8,128)} %second_gate.1) | copy-start | bytes 393220
  0.6 110.2 %copy-start.2 = (f32[32,1024]{1,0:T(8,128)S(1)}, f32[32,1024]{1,0:T(8,128)}, u32[]{:S(2)}) copy-start(f32[32,1024]{1,0:T(8,128)} %second_rec.1) | copy-start | bytes 393220
  0.7 110.2 %copy-start.1 = (f32[32,1024]{1,0:T(8,128)S(1)}, f32[32,1024]{1,0:T(8,128)}, u32[]{:S(2)}) copy-start(f32[32,1024]{1,0:T(8,128)} %first_gate.1) | copy-start | bytes 393220
  0.7 110.2 %copy-start = (f32[32,1024]{1,0:T(8,128)S(1)}, f32[32,1024]{1,0:T(8,128)}, u32[]{:S(2)}) copy-start(f32[32,1024]{1,0:T(8,128)} %first_rec.1) | copy-start | bytes 393220
